TPU v7x, 32 devices: a whole 2x2x4 slice. The times are simulated.
32 devices in a mesh: sp: 16 (over z, y, x), tp: 2 (over core).
Axes of the slice: x: 2, y: 2, z: 4, core: 2. Of those that a mesh axis runs over, the one named last changes fastest.
Arguments:
- tokens: bfloat16 [4096, 2048], P('sp', 'tp'), may hold values from -6 to 6
- norm_gain: float32 [2048], replicated, may hold values from 0.1 to 1.9
- glu_value: bfloat16 [2048, 2048], P('sp', 'tp'), may hold values from -0.125 to 0.125
- glu_gate: bfloat16 [2048, 2048], P('sp', 'tp'), may hold values from -0.125 to 0.125
- conv_taps: float32 [31, 2048], P(None, 'tp'), may hold values from -11 to 11
- ln_gain: float32 [2048], P('tp'), may hold values from 0.1 to 1.9
- ln_bias: float32 [2048], P('tp'), may hold values from -3 to 3
- query_weight: bfloat16 [2048, 2048], P('sp', 'tp'), may hold values from -0.125 to 0.125
- key_weight: bfloat16 [2048, 2048], P('sp', 'tp'), may hold values from -0.125 to 0.125
- value_weight: bfloat16 [2048, 2048], P('sp', 'tp'), may hold values from -0.125 to 0.125
- gate_weight: bfloat16 [2048, 32], replicated, may hold values from -0.125 to 0.125
- gate_bias: float32 [32], replicated, may hold values from -1 to 110
- log_decay_extra: float32 [4096, 16], P('sp'), may hold values from -1.3 to 0
- mem_gain: float32 [2048], P('tp'), may hold values from 0.1 to 1.9
- out_conv: bfloat16 [2048, 2048], P('tp'), may hold values from -0.125 to 0.125
- out_mem: bfloat16 [2048, 2048], P('tp'), may hold values from -0.125 to 0.125
Outputs:
- mixed: bfloat16 [4096, 2048], P(('sp', 'tp'))
All inputs are finite; a program needn't handle non-finite values.
Results may differ from a plain program's by a relative error of at most 0.015.
Values may be sent and summed in bfloat16 or wider, within the bound.
A program may use at most 128 MiB of HBM per device.

v0:
```python
import jax
import jax.numpy as jnp
from jax import lax
from jax.sharding import PartitionSpec as P

CONV = 2048
MEMORY_HEADS = 8
HEAD = 256
KW = 31
BLOCK = 128


EPS = 1e-06
LOW_START = -1e30
PRECISE = lax.Precision.HIGHEST


def extended(cells, sides, width):
    for axis, dim in sides:
        count = lax.axis_size(axis)
        ends = count - 1
        head = lax.slice_in_dim(cells, 0, width, axis=dim)
        tail = lax.slice_in_dim(cells, cells.shape[dim] - width, cells.shape[dim], axis=dim)
        cells = jnp.concatenate(
            [
                lax.ppermute(tail, axis, [(i, (i + 1) % count) for i in range(ends)]),
                cells,
                lax.ppermute(head, axis, [((i + 1) % count, i) for i in range(ends)]),
            ],
            axis=dim,
        )
    return cells


def prefix(part, axis, combine, identity, reverse):
    count = lax.axis_size(axis)
    place = lax.axis_index(axis)
    ahead = count - 1 - place if reverse else place
    gathered = jax.tree.map(lambda a: lax.all_gather(a, axis), part)
    state = jax.tree.map(lambda a, e: jnp.zeros_like(a) + jnp.asarray(e, a.dtype), part, identity)

    def one(hop, state):
        source = count - 1 - hop if reverse else hop
        return combine(
            state, jax.tree.map(lambda a: lax.dynamic_index_in_dim(a, source, 0, False), gathered)
        )

    return lax.fori_loop(0, ahead, one, state)


def block_step(carried_state, block_data):
    state_mat, state_vec, stabilizer = carried_state
    queries, key_rows, value_rows, input_gate, log_forget = block_data
    key_scale = HEAD ** (-0.5)
    length = log_forget.shape[-1]
    causal = jnp.tril(jnp.ones((length, length), dtype=bool))
    decay_sum = jnp.cumsum(log_forget, axis=-1)
    log_weight = jnp.where(
        causal, decay_sum[:, :, None] - decay_sum[:, None, :] + input_gate[:, None, :], -jnp.inf
    )
    carried = decay_sum + stabilizer[:, None]
    running = jnp.maximum(carried, jnp.max(log_weight, axis=-1))
    inner_weight = jnp.exp(log_weight - running[:, :, None])
    carry_weight = jnp.exp(carried - running)
    raw_scores = jnp.einsum("htd,hsd->hts", queries, key_rows, preferred_element_type=jnp.float32)
    scores = raw_scores * key_scale * inner_weight
    query_wide = queries.astype(jnp.float32)
    numerator = carry_weight[:, :, None] * jnp.einsum(
        "htd,hde->hte", query_wide, state_mat, precision=PRECISE
    )
    numerator = numerator + jnp.einsum(
        "hts,hse->hte", scores.astype(jnp.bfloat16), value_rows, preferred_element_type=jnp.float32
    )
    denominator = carry_weight * jnp.einsum(
        "htd,hd->ht", query_wide, state_vec, precision=PRECISE
    ) + jnp.sum(scores, axis=-1)
    to_end = decay_sum[:, -1:] - decay_sum + input_gate
    carried_end = decay_sum[:, -1] + stabilizer
    new_stabilizer = jnp.maximum(carried_end, jnp.max(to_end, axis=-1))
    end_weight = jnp.exp(to_end - new_stabilizer[:, None]) * key_scale
    keep_weight = jnp.exp(carried_end - new_stabilizer)
    weighted = key_rows.astype(jnp.float32) * end_weight[:, :, None]
    new_mat = keep_weight[:, None, None] * state_mat + jnp.einsum(
        "hsd,hse->hde",
        weighted.astype(jnp.bfloat16),
        value_rows,
        preferred_element_type=jnp.float32,
    )
    new_vec = keep_weight[:, None] * state_vec + jnp.sum(weighted, axis=1)
    return ((new_mat, new_vec, new_stabilizer), (numerator, denominator, running, decay_sum))


def local_pass(queries, key_rows, value_rows, input_gate, log_forget):
    head_count, length, head_width = queries.shape
    count = length // BLOCK

    def blocked(tensor):
        return jnp.moveaxis(tensor.reshape((head_count, count, BLOCK) + tensor.shape[2:]), 1, 0)

    def unblocked(tensor):
        return jnp.moveaxis(tensor, 0, 1).reshape((head_count, length) + tensor.shape[3:])

    start = (
        jnp.zeros((head_count, head_width, head_width), jnp.float32),
        jnp.zeros((head_count, head_width), jnp.float32),
        jnp.full((head_count,), LOW_START, jnp.float32),
    )
    final, outputs = lax.scan(
        block_step,
        start,
        (
            blocked(queries),
            blocked(key_rows),
            blocked(value_rows),
            blocked(input_gate),
            blocked(log_forget),
        ),
    )
    numerator, denominator, running, decay_sum = outputs
    totals = decay_sum[:, :, -1]
    offsets = jnp.cumsum(totals, axis=0) - totals
    decay_sum = decay_sum + offsets[:, :, None]
    summary = (offsets[-1] + totals[-1], final[0], final[1], final[2])
    return (
        unblocked(numerator),
        unblocked(denominator),
        unblocked(running),
        unblocked(decay_sum),
        summary,
    )


def compose(earlier, later):
    early_decay, early_mat, early_vec, early_level = earlier
    late_decay, late_mat, late_vec, late_level = later
    stabilizer = jnp.maximum(early_level + late_decay, late_level)
    early_weight = jnp.exp(early_level + late_decay - stabilizer)
    late_weight = jnp.exp(late_level - stabilizer)
    return (
        early_decay + late_decay,
        early_weight[:, None, None] * early_mat + late_weight[:, None, None] * late_mat,
        early_weight[:, None] * early_vec + late_weight[:, None] * late_vec,
        stabilizer,
    )


def finish(queries, numerator, denominator, running, decay_sum, incoming):
    in_mat, in_vec, in_level = (incoming[1], incoming[2], incoming[3])
    query_wide = queries.astype(jnp.float32)
    carried = decay_sum + in_level[:, None]
    stabilizer = jnp.maximum(running, carried)
    local_weight = jnp.exp(running - stabilizer)
    carry_weight = jnp.exp(carried - stabilizer)
    numerator = local_weight[:, :, None] * numerator
    numerator = numerator + carry_weight[:, :, None] * jnp.einsum(
        "htd,hde->hte", query_wide, in_mat, precision=PRECISE
    )
    denominator = local_weight * denominator + carry_weight * jnp.einsum(
        "htd,hd->ht", query_wide, in_vec, precision=PRECISE
    )
    return numerator / jnp.maximum(jnp.abs(denominator), jnp.exp(-stabilizer))[:, :, None]


def shards(
    tokens,
    norm_gain,
    glu_value,
    glu_gate,
    conv_taps,
    ln_gain,
    ln_bias,
    query_weight,
    key_weight,
    value_weight,
    gate_weight,
    gate_bias,
    log_decay_extra,
    mem_gain,
    out_conv,
    out_mem,
):
    whole_rows = lax.all_gather(tokens, "tp", axis=1, tiled=True)
    wide = whole_rows.astype(jnp.float32)
    normed = (
        wide * lax.rsqrt(jnp.mean(wide * wide, axis=-1, keepdims=True) + EPS) * norm_gain
    ).astype(jnp.bfloat16)
    row_count = normed.shape[0]
    head_count = mem_gain.shape[0] // HEAD
    first_head = lax.axis_index("tp") * head_count
    gate_all = (
        jnp.dot(normed, gate_weight, preferred_element_type=jnp.float32) + gate_bias
    ).reshape(row_count, 4, MEMORY_HEADS)
    own_gates = lax.dynamic_slice_in_dim(gate_all, first_head, head_count, 2)
    own_extra = lax.dynamic_slice_in_dim(
        log_decay_extra.reshape(row_count, 2, MEMORY_HEADS), first_head, head_count, 2
    )

    def fold_rows(pieces):
        return tuple(
            (
                jnp.dot(normed, weight_rows, preferred_element_type=jnp.float32)
                for weight_rows in pieces
            )
        )

    def memory_branch(query_proj, key_proj, value_proj):

        def head_major(tensor):
            return jnp.transpose(tensor.reshape(row_count, head_count, HEAD), (1, 0, 2))

        queries = head_major(query_proj)
        key_rows = head_major(key_proj)
        value_rows = head_major(value_proj)
        input_fwd = own_gates[:, 0, :].T
        forget_fwd = (jax.nn.log_sigmoid(own_gates[:, 1, :]) + own_extra[:, 0, :]).T
        input_bwd = own_gates[:, 2, :].T
        forget_bwd = (jax.nn.log_sigmoid(own_gates[:, 3, :]) + own_extra[:, 1, :]).T
        identity = (
            jnp.zeros((head_count,), jnp.float32),
            jnp.zeros((head_count, HEAD, HEAD), jnp.float32),
            jnp.zeros((head_count, HEAD), jnp.float32),
            jnp.full((head_count,), LOW_START, jnp.float32),
        )
        numerator, denominator, running, decay_sum, summary = local_pass(
            queries, key_rows, value_rows, input_fwd, forget_fwd
        )
        incoming = prefix(summary, "sp", compose, identity, False)
        forward_out = finish(queries, numerator, denominator, running, decay_sum, incoming)
        back_queries = jnp.flip(queries, 1)
        numerator, denominator, running, decay_sum, summary = local_pass(
            back_queries,
            jnp.flip(key_rows, 1),
            jnp.flip(value_rows, 1),
            jnp.flip(input_bwd, 1),
            jnp.flip(forget_bwd, 1),
        )
        incoming = prefix(summary, "sp", compose, identity, True)
        backward_out = jnp.flip(
            finish(back_queries, numerator, denominator, running, decay_sum, incoming), 1
        )
        summed = forward_out + backward_out
        head_norm = summed * lax.rsqrt(jnp.mean(summed * summed, axis=-1, keepdims=True) + EPS)
        head_norm = head_norm * mem_gain.reshape(head_count, HEAD)[:, None, :]
        return (
            jnp.transpose(head_norm, (1, 0, 2))
            .reshape(row_count, head_count * HEAD)
            .astype(jnp.bfloat16)
        )

    sums = fold_rows(
        (
            lax.all_gather(glu_value, "sp", axis=0, tiled=True),
            lax.all_gather(glu_gate, "sp", axis=0, tiled=True),
        )
    )
    glu = (sums[0] * jax.nn.sigmoid(sums[1])).astype(jnp.bfloat16)
    reach = KW // 2
    padded = extended(glu, (("sp", 0),), reach).astype(jnp.float32)
    conv = jnp.zeros(glu.shape, jnp.float32)
    for offset in range(KW):
        conv = conv + conv_taps[offset] * padded[offset : offset + row_count]
    chan_sums = jnp.sum(conv, axis=-1)
    chan_squares = jnp.sum(conv * conv, axis=-1)
    chan_sums, chan_squares = lax.psum((chan_sums, chan_squares), "tp")
    chan_mean = chan_sums / CONV
    chan_var = chan_squares / CONV - chan_mean * chan_mean
    normal = (conv - chan_mean[:, None]) * lax.rsqrt(chan_var + EPS)[:, None] * ln_gain + ln_bias
    act = (normal * jax.nn.sigmoid(normal)).astype(jnp.bfloat16)
    sums = fold_rows(
        (
            lax.all_gather(query_weight, "sp", axis=0, tiled=True),
            lax.all_gather(key_weight, "sp", axis=0, tiled=True),
            lax.all_gather(value_weight, "sp", axis=0, tiled=True),
        )
    )
    memory = memory_branch(*tuple((projected.astype(jnp.bfloat16) for projected in sums)))
    result = jnp.dot(act, out_conv, preferred_element_type=jnp.float32)
    return lax.psum_scatter(
        (result + jnp.dot(memory, out_mem, preferred_element_type=jnp.float32)).astype(
            jnp.bfloat16
        ),
        "tp",
        scatter_dimension=0,
        tiled=True,
    )


def solution(mesh):
    in_specs = (
        P("sp", "tp"),
        P(),
        P("sp", "tp"),
        P("sp", "tp"),
        P(None, "tp"),
        P("tp"),
        P("tp"),
        P("sp", "tp"),
        P("sp", "tp"),
        P("sp", "tp"),
        P(),
        P(),
        P("sp", None),
        P("tp"),
        P("tp", None),
        P("tp", None),
    )
    out_specs = P(("sp", "tp"), None)
    return jax.shard_map(shards, mesh=mesh, in_specs=in_specs, out_specs=out_specs, check_vma=False)
```

profile of v0, /device:TPU:0, one launch (start us, length us, event | category | flops | bytes accessed | tf_op | source)
XLA Modules:
  0.0 853.2 jit_solution(16429110162480425657)
XLA Ops:
  10.6 10.1 %all-gather.19.cloned.1.call-done = bf16[256,2048]{1,0:T(8,128)(2,1)} async-done(((bf16[256,1024]{1,0:T(8,128)(2,1)}), bf16[256,2048]{1,0:T(8,128)(2,1)}) %all-gather.19.cloned.1.call-update) | async-done | bytes 1048592 | tf_op jit(solution)/shard_map/all_gather | solution.py:182
  22.3 1.7 fusion.103
  24.1 76.2 %all-gather.29.cloned.1.call-done = bf16[2048,1024]{1,0:T(8,128)(2,1)} async-done(((bf16[128,1024]{1,0:T(8,128)(2,1)}), bf16[2048,1024]{1,0:T(8,128)(2,1)}) %all-gather.29.cloned.1.call-update) | async-done | bytes 4194320 | tf_op jit(solution)/shard_map/all_gather | solution.py:271
  100.2 3.5 convolution_convert_fusion
  103.8 73.5 %all-gather.25.cloned.1.call-done = bf16[2048,1024]{1,0:T(8,128)(2,1)} async-done(((bf16[128,1024]{1,0:T(8,128)(2,1)}), bf16[2048,1024]{1,0:T(8,128)(2,1)}) %all-gather.25.cloned.1.call-update) | async-done | bytes 4194320 | tf_op jit(solution)/shard_map/all_gather | solution.py:272
  177.2 3.5 convolution_convert_fusion.2
  180.8 73.3 %all-gather.27.cloned.1.call-done = bf16[2048,1024]{1,0:T(8,128)(2,1)} async-done(((bf16[128,1024]{1,0:T(8,128)(2,1)}), bf16[2048,1024]{1,0:T(8,128)(2,1)}) %all-gather.27.cloned.1.call-update) | async-done | bytes 4194320 | tf_op jit(solution)/shard_map/all_gather | solution.py:273
  254.1 3.8 convolution_convert_fusion.1
  259.0 7.6 while.82
  271.2 7.5 while.83
  281.7 40.6 %all-reduce.2 = (f32[64]{0:T(128)S(1)}, f32[64]{0:T(128)S(1)}) all-reduce(f32[64]{0:T(128)S(1)} %dynamic-update-slice.1, f32[64]{0:T(128)S(1)} %dynamic-update-slice), channel_id=5, replica_groups=mesh['sp'=16,'tp'=2] {'sp'}, use_global_device_ids=true, to_apply=%add.1 | all-reduce | flops 128 | bytes 1024
  323.9 3.1 reshape.473
  327.6 1.8 reshape.464
  329.3 2.0 all-gather.23.cloned.1.call-done
  331.4 4.5 fusion.101
  335.9 72.5 %all-gather.21.cloned.1.call-done = bf16[2048,1024]{1,0:T(8,128)(2,1)} async-done(((bf16[128,1024]{1,0:T(8,128)(2,1)}), bf16[2048,1024]{1,0:T(8,128)(2,1)}) %all-gather.21.cloned.1.call-update) | async-done | bytes 4194320 | tf_op jit(solution)/shard_map/all_gather | solution.py:252
  408.5 3.8 fusion.102
  412.3 3.3 collective-permute-start
  417.2 40.5 %all-gather.6 = f32[16,1,4]{2,1,0:T(1,128)S(1)} all-gather(f32[1,1,4]{2,1,0:T(1,128)S(1)} %fusion.163), channel_id=1, replica_groups=mesh['sp'=16,'tp'=2] {'sp'}, dimensions={0}, use_global_device_ids=true | all-gather | bytes 272 | tf_op jit(solution)/shard_map/all_gather | solution.py:39
  457.9 36.7 %all-gather.8 = f32[16,1,4]{2,1,0:T(1,128)S(1)} all-gather(f32[1,1,4]{2,1,0:T(1,128)S(1)} %fusion.162), channel_id=1, replica_groups=mesh['sp'=16,'tp'=2] {'sp'}, dimensions={0}, use_global_device_ids=true | all-gather | bytes 272 | tf_op jit(solution)/shard_map/all_gather | solution.py:39
  494.6 39.4 %all-gather.7 = f32[16,4,256]{2,1,0:T(4,128)S(1)} all-gather(f32[1,4,256]{2,1,0:T(4,128)S(1)} %bitcast.542), channel_id=4, replica_groups=mesh['sp'=16,'tp'=2] {'sp'}, dimensions={0}, use_global_device_ids=true | all-gather | bytes 69632 | tf_op jit(solution)/shard_map/all_gather | solution.py:39
  534.0 37.8 %all-gather.9 = f32[16,4,256]{2,1,0:T(4,128)S(1)} all-gather(f32[1,4,256]{2,1,0:T(4,128)S(1)} %bitcast.543), channel_id=7, replica_groups=mesh['sp'=16,'tp'=2] {'sp'}, dimensions={0}, use_global_device_ids=true | all-gather | bytes 69632 | tf_op jit(solution)/shard_map/all_gather | solution.py:39
  572.1 5.8 fusion.178
  577.8 2.5 all-reduce.3
  580.3 5.0 fusion.134
  585.4 17.7 %all-gather.31.cloned.1.call-done = f32[64,256,256]{2,1,0:T(8,128)} async-done(((f32[4,256,256]{2,1,0:T(8,128)}), f32[64,256,256]{2,1,0:T(8,128)}) %all-gather.31.cloned.1.call-update) | async-done | bytes 16777232 | tf_op jit(solution)/shard_map/all_gather | solution.py:39
  604.7 190.5 %all-gather.33.cloned.1.call-done = f32[64,256,256]{2,1,0:T(8,128)} async-done(((f32[4,256,256]{2,1,0:T(8,128)}), f32[64,256,256]{2,1,0:T(8,128)}) %all-gather.33.cloned.1.call-update) | async-done | bytes 16777232 | tf_op jit(solution)/shard_map/all_gather | solution.py:39
  795.3 28.0 %while.81 = (s32[]{:T(128)}, f32[4,256,256]{2,1,0:T(8,128)S(1)}, f32[4,256]{1,0:T(4,128)S(1)}, f32[4]{0:T(128)S(1)}, s32[]{:T(128)}, /*index=5*/f32[16,4]{1,0:T(...) while((s32[]{:T(128)}, f32[4,256,256]{2,1,0:T(8,128)S(1)}, ...), condition=%wide.region_24.25_spmd, body=%wide.region_23.24_spmd.sunk | while | flops 789526 | bytes 3158395 | solution.py:48
  795.4 1.7 fusion.246
  797.3 1.7 fusion.246
  799.1 1.7 fusion.246
  801.0 1.7 fusion.246
  802.8 1.7 fusion.246
  804.7 1.7 fusion.246
  806.5 1.7 fusion.246
  808.4 1.7 fusion.246
  810.2 1.7 fusion.246
  812.1 1.7 fusion.246
  813.9 1.7 fusion.246
  815.8 1.7 fusion.246
  817.6 1.7 fusion.246
  819.5 1.7 fusion.246
  821.3 1.7 fusion.246
  823.9 3.3 fusion.95
  827.2 9.4 %rev.26 = f32[4,256,256]{1,2,0:T(8,128)} reverse(f32[4,256,256]{1,2,0:T(8,128)} %fusion.95), dimensions={1} | reverse | bytes 2097152 | tf_op jit(solution)/shard_map/jit(_flip)/rev | solution.py:238
  836.8 2.5 multiply_reduce_fusion
  840.0 2.3 fusion.90
  842.2 4.4 reduce-scatter.2.cloned.1.call-done
  (260 shorter events, 37.2 us)
Async XLA Ops:
  6.5 15.7 %copy-start = (bf16[2048,32]{0,1:T(8,128)(2,1)S(1)}, bf16[2048,32]{0,1:T(8,128)(2,1)}, u32[]{:S(2)}) copy-start(bf16[2048,32]{0,1:T(8,128)(2,1)} %param.34) | copy-start | bytes 393220
  6.5 15.8 %copy-start.19 = (f32[2048]{0:T(1024)S(1)}, f32[2048]{0:T(1024)}, u32[]{:S(2)}) copy-start(f32[2048]{0:T(1024)} %param.25) | copy-start | bytes 24580
  6.5 15.8 %copy-start.22 = (f32[32]{0:T(128)S(1)}, f32[32]{0:T(128)}, u32[]{:S(2)}) copy-start(f32[32]{0:T(128)} %param.35) | copy-start | bytes 388
  6.5 14.1 %all-gather.19.cloned.1.call-start = ((), (), s32[]{:S(2)}) async-start(), calls=%async_computation.1 | async-start | bytes 1572864 | tf_op jit(solution)/shard_map/all_gather | solution.py:182
  7.3 93.0 %all-gather.29.cloned.1.call-start = ((), (), s32[]{:S(2)}) async-start(), calls=%async_computation.6 | async-start | bytes 4456448 | tf_op jit(solution)/shard_map/all_gather | solution.py:271
  8.0 16.0 %copy-start.16 = (f32[256,16]{0,1:T(8,128)S(1)}, f32[256,16]{0,1:T(8,128)}, u32[]{:S(2)}) copy-start(f32[256,16]{0,1:T(8,128)} %param.36) | copy-start | bytes 49156
  8.0 169.2 %all-gather.25.cloned.1.call-start = ((), (), s32[]{:S(2)}) async-start(), calls=%async_computation.4 | async-start | bytes 4456448 | tf_op jit(solution)/shard_map/all_gather | solution.py:272
  8.8 245.3 %all-gather.27.cloned.1.call-start = ((), (), s32[]{:S(2)}) async-start(), calls=%async_computation.5 | async-start | bytes 4456448 | tf_op jit(solution)/shard_map/all_gather | solution.py:273
  9.3 322.0 %all-gather.23.cloned.1.call-start = ((), (), s32[]{:S(2)}) async-start(), calls=%async_computation.3 | async-start | bytes 4456448 | tf_op jit(solution)/shard_map/all_gather | solution.py:253
  9.9 398.5 %all-gather.21.cloned.1.call-start = ((), (), s32[]{:S(2)}) async-start(), calls=%async_computation.2 | async-start | bytes 4456448 | tf_op jit(solution)/shard_map/all_gather | solution.py:252
  10.5 592.6 %all-gather.31.cloned.1.call-start = ((), (), s32[]{:S(2)}) async-start(), calls=%async_computation.8 | async-start | bytes 17825792 | tf_op jit(solution)/shard_map/all_gather | solution.py:39
  20.7 79.6 %copy-start.10 = (bf16[256,2048]{1,0:T(8,128)(2,1)S(1)}, bf16[256,2048]{1,0:T(8,128)(2,1)}, u32[]{:S(2)}) copy-start(bf16[256,2048]{1,0:T(8,128)(2,1)} %all-gather.19.cloned.1.call-done) | copy-start | bytes 3145732
  103.7 77.0 %copy-start.13 = (bf16[256,1024]{1,0:T(8,128)(2,1)}, bf16[256,1024]{1,0:T(8,128)(2,1)S(1)}, u32[]{:S(2)}) copy-start(bf16[256,1024]{1,0:T(8,128)(2,1)S(1)} %convolution_convert_fusion) | copy-start | bytes 1572868
  260.0 1.3 copy-start.4
  261.8 1.0 copy-start.5
  263.8 1.3 copy-start.4
  265.6 1.0 copy-start.5
  266.6 1.1 copy-start.2
  267.7 527.5 %all-gather.33.cloned.1.call-start = ((), (), s32[]{:S(2)}) async-start(), calls=%async_computation.9 | async-start | bytes 17825792 | tf_op jit(solution)/shard_map/all_gather | solution.py:39
  271.2 8.6 %copy-start.17 = (f32[1024]{0:T(1024)S(1)}, f32[1024]{0:T(1024)}, u32[]{:S(2)}) copy-start(f32[1024]{0:T(1024)} %param.37) | copy-start | bytes 12292
  271.2 8.6 %copy-start.23 = (u32[32]{0:T(128)S(1)}, u32[32]{0:T(128)}, u32[]{:S(2)}) copy-start(u32[32]{0:T(128)} %constant.164) | copy-start | bytes 388
  271.2 9.8 %copy-start.15 = (f32[31,1024]{1,0:T(8,128)S(1)}, f32[31,1024]{1,0:T(8,128)}, u32[]{:S(2)}) copy-start(f32[31,1024]{1,0:T(8,128)} %param.28) | copy-start | bytes 380932
  272.1 1.3 copy-start.7
  274.0 1.0 copy-start.8
  275.9 1.3 copy-start.7
  277.7 1.0 copy-start.8
  278.7 1.0 copy-start.3
  278.7 43.9 %copy-start.9 = (f32[2,4,128,256]{3,2,1,0:T(8,128)S(1)}, f32[2,4,128,256]{3,2,1,0:T(8,128)}, u32[]{:S(2)}) copy-start(f32[2,4,128,256]{3,2,1,0:T(8,128)} %get-tuple-element.383) | copy-start | bytes 3145732
  279.6 567.0 %reduce-scatter.2.cloned.1.call-start = ((), (), s32[]{:S(2)}) async-start(), calls=%async_computation.7 | async-start | bytes 1572864 | tf_op jit(solution)/shard_map/reduce_scatter | solution.py:278
  322.6 4.3 copy-start.6
  327.5 3.8 copy-start.11
  412.3 159.6 %collective-permute-start = (bf16[15,1024]{1,0:T(8,128)(2,1)S(1)}, bf16[15,1024]{1,0:T(8,128)(2,1)S(1)}, u32[]{:S(2)}, u32[]{:S(2)}) collective-permute-start(bf16[15,1024]{1,0:T(8,128)(2,1)S(1)} %get-tuple-element.714), channel_id=1, source_target_pairs={{0,2},{2,4},{4,6},{6,8},{8,10},{10,12},{12,14},{14,16},{16,18},{18... | collective-permute-start | bytes 92168 | tf_op jit(solution)/shard_map/ppermute | solution.py:26
  415.6 156.2 %collective-permute-start.1 = (bf16[15,1024]{1,0:T(8,128)(2,1)S(1)}, bf16[15,1024]{1,0:T(8,128)(2,1)S(1)}, u32[]{:S(2)}, u32[]{:S(2)}) collective-permute-start(bf16[15,1024]{1,0:T(8,128)(2,1)S(1)} %get-tuple-element.715), channel_id=1, source_target_pairs={{2,0},{4,2},{6,4},{8,6},{10,8},{12,10},{14,12},{16,14},{18,16},{20... | collective-permute-start | bytes 92168 | tf_op jit(solution)/shard_map/ppermute | solution.py:28
  572.0 8.3 copy-start.20
  572.1 8.3 copy-start.21
  603.2 1.0 copy-start.14
  827.2 9.5 %copy-start.12 = (f32[4,256,256]{1,2,0:T(8,128)S(1)}, f32[4,256,256]{1,2,0:T(8,128)}, u32[]{:S(2)}) copy-start(f32[4,256,256]{1,2,0:T(8,128)} %reshape.464) | copy-start | bytes 3145732
  836.8 2.8 copy-start.18
  836.8 3.2 copy-start.24
  839.9 6.7 copy-start.1
Sparse Core Ops, SparseCore 0:
  8.9 11.7 all-gather.18
  23.4 76.7 all-gather.28
  103.0 74.1 all-gather.24
  179.9 74.1 all-gather.26
  256.7 74.6 all-gather.22
  334.0 74.4 all-gather.20
  411.2 191.7 all-gather.30
  605.8 189.3 all-gather.32
  842.4 4.2 reduce-scatter.1
where the time goes:
time: 855 us; the launch traced here: 853 us
  waiting for transfers between devices  524 us (61%)
  blocking collectives  197 us (23%)
  matrix products  42.8 us (5%)
  other arithmetic  40.3 us (5%)
  local copies, waits for them, and re-layouts  28.7 us (3%)
  between operations  14.4 us (2%)
    all_gather x2, waiting for transfers between devices, prefix(): gathered = jax.tree.map(lambda a: lax.all_gather(a, axis), part)  208 us
    all_gather x4, blocking collectives, prefix(): gathered = jax.tree.map(lambda a: lax.all_gather(a, axis), part)  154 us
    all_gather x1, waiting for transfers between devices, shards(): lax.all_gather(query_weight, 'sp', axis=0, tiled=True)  76.2 us
    all_gather x1, waiting for transfers between devices, shards(): lax.all_gather(key_weight, 'sp', axis=0, tiled=True)  73.5 us
    all_gather x1, waiting for transfers between devices, shards(): lax.all_gather(value_weight, 'sp', axis=0, tiled=True)  73.3 us
    all_gather x1, waiting for transfers between devices, shards(): lax.all_gather(glu_value, 'sp', axis=0, tiled=True)  72.5 us
    unnamed x1, blocking collectives  40.6 us
    add x15, other arithmetic, compose(): early_weight[:, None, None] * early_mat  25.9 us
  transfers between devices with their start and end apart: 11, of which 9 were waited for; matrix products, arithmetic and copies ran while one was open for 7% of the time, Pallas kernels for 0%

commit v1 on v0

v1 whole, which is shorter than its diff:
```python
import math

import jax
import jax.numpy as jnp
from jax import lax
from jax.sharding import Mesh, PartitionSpec as P

MEMORY_HEADS = 8
HEAD = 256
KW = 31

EPS = 1e-06
PRECISE = lax.Precision.HIGHEST


def parts_of(x):
    first = lax.reduce_precision(x, 8, 7)
    rest = x - first
    second = lax.reduce_precision(rest, 8, 7)
    third = rest - second
    return [p.astype(jnp.bfloat16) for p in (first, second, third)]


def whole_of(a, b, c):
    return a.astype(jnp.float32) + b.astype(jnp.float32) + c.astype(jnp.float32)


def gather_inputs(tokens, weights, extra, inner):
    rows, half = tokens.shape
    gathered = lax.all_gather(tokens, ("inner", "tp"), axis=0)
    tp = gathered.shape[0] // inner
    whole = jnp.transpose(gathered.reshape(inner, tp, rows, half), (0, 2, 1, 3))
    whole = whole.reshape(inner * rows, tp * half)
    depth, columns = weights[0].shape
    width = columns // inner
    packed = jnp.stack([w.reshape(depth, inner, width) for w in weights], axis=2)
    packed = jnp.transpose(packed, (1, 0, 2, 3)).reshape(inner, depth, len(weights) * width)
    if inner > 1:
        packed = lax.all_to_all(packed, "inner", split_axis=0, concat_axis=0, tiled=True)
    pieces = lax.all_gather(packed.reshape(inner * depth, -1), "outer", axis=0, tiled=True)
    extras = lax.all_gather(extra, "inner", axis=0, tiled=True) if inner > 1 else extra
    return whole, pieces, extras


def local_state(keys, values, shifted, level, total, scale):
    weight = jnp.exp(shifted - level[:, None]) * scale
    weighted = keys.astype(jnp.float32) * weight[:, :, None]
    mat = jnp.einsum(
        "hsd,hse->hde", weighted.astype(jnp.bfloat16), values, preferred_element_type=jnp.float32
    )
    return mat, jnp.sum(weighted, axis=1), level + total, total


def packed_state(mat, vec, level, decay):
    spread = lambda x: jnp.broadcast_to(x[:, None], vec.shape)
    rows = parts_of(vec) + parts_of(spread(level)) + parts_of(spread(decay))
    pad = [jnp.zeros_like(rows[0])] * 7
    return jnp.concatenate([mat.astype(jnp.bfloat16), jnp.stack(rows + pad, axis=1)], axis=1)


def incoming(states, reverse):
    count = states.shape[0]
    mats = states[:, :, :HEAD]
    rows = states[:, :, HEAD:]
    vecs = whole_of(rows[:, :, 0], rows[:, :, 1], rows[:, :, 2])
    levels = whole_of(rows[:, :, 3, 0], rows[:, :, 4, 0], rows[:, :, 5, 0])
    decays = whole_of(rows[:, :, 6, 0], rows[:, :, 7, 0], rows[:, :, 8, 0])
    place = lax.axis_index("outer")
    order = jnp.arange(count)
    if reverse:
        ahead = (order > place)[:, None]
        between = (order[None, :] < order[:, None]) & (order[None, :] > place)
    else:
        ahead = (order < place)[:, None]
        between = (order[None, :] > order[:, None]) & (order[None, :] < place)
    lost = jnp.sum(jnp.where(between[:, :, None], decays[None], 0.0), axis=1)
    reach = jnp.where(ahead, levels + lost, -1e30)
    level = jnp.max(reach, axis=0)
    share = jnp.where(ahead, jnp.exp(reach - level[None]), 0.0)
    mat = jnp.sum(share[:, :, None, None] * mats.astype(jnp.float32), axis=0)
    vec = jnp.sum(share[:, :, None] * vecs, axis=0)
    return mat, vec, level


def finish(query_wide, num, den, running, decay, state):
    mat, vec, level = state
    top = jnp.maximum(running, level[:, None])
    local_weight = jnp.exp(running - top)
    carry_weight = jnp.exp(level[:, None] - top)
    num = local_weight[:, :, None] * num + carry_weight[:, :, None] * jnp.einsum(
        "htd,hde->hte", query_wide, mat, precision=PRECISE
    )
    den = local_weight * den + carry_weight * jnp.einsum(
        "htd,hd->ht", query_wide, vec, precision=PRECISE
    )
    return num / jnp.maximum(jnp.abs(den), jnp.exp(-top - decay))[:, :, None]


def make_shards(inner, outer, tp):
    def own(array, dim):
        size = array.shape[dim] // inner
        return lax.dynamic_slice_in_dim(array, lax.axis_index("inner") * size, size, dim)

    def shards(
        tokens,
        norm_gain,
        glu_value,
        glu_gate,
        conv_taps,
        ln_gain,
        ln_bias,
        query_weight,
        key_weight,
        value_weight,
        gate_weight,
        gate_bias,
        log_decay_extra,
        mem_gain,
        out_conv,
        out_mem,
    ):
        taps, gain, bias, mgain = own(conv_taps, 1), own(ln_gain, 0), own(ln_bias, 0), own(mem_gain, 0)
        channels = conv_taps.shape[1] * tp
        width = gain.shape[0]
        heads = mgain.shape[0] // HEAD
        first = (lax.axis_index("tp") * inner + lax.axis_index("inner")) * heads
        whole, weights, extras = gather_inputs(
            tokens, (query_weight, key_weight, value_weight, glu_value, glu_gate),
            log_decay_extra, inner,
        )
        rows = whole.shape[0]
        wide = whole.astype(jnp.float32)
        normed = (
            wide * lax.rsqrt(jnp.mean(wide * wide, axis=-1, keepdims=True) + EPS) * norm_gain
        ).astype(jnp.bfloat16)
        own_gate = lax.dynamic_slice_in_dim(
            gate_weight.reshape(-1, 4, MEMORY_HEADS), first, heads, 2
        )
        own_bias = lax.dynamic_slice_in_dim(gate_bias.reshape(4, MEMORY_HEADS), first, heads, 1)
        gates = lax.dot_general(
            own_gate.reshape(-1, 4 * heads), normed, (((0,), (1,)), ((), ())),
            preferred_element_type=jnp.float32,
        ).reshape(4, heads, rows) + own_bias[:, :, None]
        own_extra = lax.dynamic_slice_in_dim(
            extras.reshape(rows, 2, MEMORY_HEADS), first, heads, 2
        ).transpose(1, 2, 0)
        lf = jax.nn.log_sigmoid(gates[1::2]) + own_extra
        decay_f = jnp.cumsum(lf[0], axis=-1)
        decay_b = lax.cumsum(lf[1], axis=1, reverse=True)
        shifted_f = gates[0] - decay_f
        shifted_b = gates[2] - decay_b
        running_f = lax.cummax(shifted_f, axis=1)
        running_b = lax.cummax(shifted_b, axis=1, reverse=True)

        def project(i):
            return jnp.dot(
                normed, weights[:, i * width : (i + 1) * width],
                preferred_element_type=jnp.float32,
            )

        def heads_first(x):
            return jnp.transpose(x.reshape(rows, heads, HEAD), (1, 0, 2)).astype(jnp.bfloat16)

        keys = heads_first(project(1))
        values = heads_first(project(2))
        scale = HEAD ** (-0.5)
        state_f = local_state(
            keys, values, shifted_f, running_f[:, -1], decay_f[:, -1], scale
        )
        state_b = local_state(keys, values, shifted_b, running_b[:, 0], decay_b[:, 0], scale)
        sent = jnp.stack([packed_state(*state_f), packed_state(*state_b)])
        states = lax.all_gather(sent, "outer", axis=0)

        glu = (project(3) * jax.nn.sigmoid(project(4))).astype(jnp.bfloat16)
        reach = KW // 2
        before = lax.ppermute(glu[rows - reach :], "outer", [(i, i + 1) for i in range(outer - 1)])
        after = lax.ppermute(glu[:reach], "outer", [(i + 1, i) for i in range(outer - 1)])
        queries = heads_first(project(0))

        scores = jnp.einsum("htd,hsd->hts", queries, keys, preferred_element_type=jnp.float32) * scale
        at = jnp.arange(rows)
        causal = at[:, None] >= at[None, :]
        anti = at[:, None] <= at[None, :]

        def local_out(shifted, running, mask):
            weight = jnp.where(
                mask, jnp.exp(jnp.minimum(shifted[:, None, :] - running[:, :, None], 0.0)), 0.0
            )
            part = scores * weight
            num = jnp.einsum(
                "hts,hse->hte", part.astype(jnp.bfloat16), values,
                preferred_element_type=jnp.float32,
            )
            return num, jnp.sum(part, axis=-1)

        num_f, den_f = local_out(shifted_f, running_f, causal)
        num_b, den_b = local_out(shifted_b, running_b, anti)

        padded = jnp.concatenate([before, glu, after], axis=0).astype(jnp.float32)
        conv = jnp.zeros(glu.shape, jnp.float32)
        for offset in range(KW):
            conv = conv + taps[offset] * padded[offset : offset + rows]
        sums = jnp.stack([jnp.sum(conv, axis=-1), jnp.sum(conv * conv, axis=-1)])
        sums = lax.psum(sums, ("inner", "tp")) / channels
        chan_mean = sums[0]
        chan_var = sums[1] - chan_mean * chan_mean
        normal = (conv - chan_mean[:, None]) * lax.rsqrt(chan_var + EPS)[:, None] * gain + bias
        act = (normal * jax.nn.sigmoid(normal)).astype(jnp.bfloat16)

        query_wide = queries.astype(jnp.float32)
        forward = finish(query_wide, num_f, den_f, running_f, decay_f, incoming(states[:, 0], False))
        backward = finish(query_wide, num_b, den_b, running_b, decay_b, incoming(states[:, 1], True))
        summed = forward + backward
        head_norm = summed * lax.rsqrt(jnp.mean(summed * summed, axis=-1, keepdims=True) + EPS)
        head_norm = head_norm * mgain.reshape(heads, HEAD)[:, None, :]
        memory = jnp.transpose(head_norm, (1, 0, 2)).reshape(rows, heads * HEAD).astype(jnp.bfloat16)

        def back(x):
            if inner == 1:
                return x
            return lax.all_to_all(x, "inner", split_axis=0, concat_axis=1, tiled=True)

        result = jnp.dot(back(act), out_conv, preferred_element_type=jnp.float32)
        result = result + jnp.dot(back(memory), out_mem, preferred_element_type=jnp.float32)
        return lax.psum_scatter(
            result.astype(jnp.bfloat16), "tp", scatter_dimension=0, tiled=True
        )

    return shards


def solution(mesh):
    sp, tp = mesh.shape["sp"], mesh.shape["tp"]
    inner = math.gcd(sp, max(MEMORY_HEADS // tp, 1))
    outer = sp // inner
    fine = Mesh(mesh.devices.reshape(outer, inner, tp), ("outer", "inner", "tp"))
    rows = ("outer", "inner")
    in_specs = (
        P(rows, "tp"),
        P(),
        P(rows, "tp"),
        P(rows, "tp"),
        P(None, "tp"),
        P("tp"),
        P("tp"),
        P(rows, "tp"),
        P(rows, "tp"),
        P(rows, "tp"),
        P(),
        P(),
        P(rows, None),
        P("tp"),
        P("tp", None),
        P("tp", None),
    )
    return jax.shard_map(
        make_shards(inner, outer, tp), mesh=fine, in_specs=in_specs,
        out_specs=P(("outer", "inner", "tp"), None), check_vma=False,
    )
```

time: 855 us -> 262 us (0.31)
  waiting for transfers between devices: 524 us -> 62.4 us
  blocking collectives: 197 us -> 50.6 us
  between operations: 14.4 us -> 33.3 us
    all_gather x8 -> x3, waiting for transfers between devices: 516 us -> 50 us  [the longest x1 43.8 us: gather_inputs(): lax.all_gather(packed.reshape(inner * depth, -1), 'outer', axis=0, tiled=...]
    all_gather x4 -> x1, blocking collectives: 154 us -> 8.41 us  [gather_inputs(): lax.all_gather(extra, 'inner', axis=0, tiled=True)]
    unnamed x1 -> x0, blocking collectives: 40.6 us -> none
    all_to_all x0 -> x1, blocking collectives: none -> 27.6 us  [gather_inputs(): lax.all_to_all(packed, 'inner', split_axis=0, concat_axis=0, tiled=True)]
    add x36 -> x3, other arithmetic: 27.3 us -> 0.28 us  [the longest x2 0.24 us: whole_of(): return a.astype(jnp.float32) + b.astype(jnp.float32) + c.astype(jnp.float32)]
    another operation x6 -> x11, other arithmetic: 1.31 us -> 13.6 us  [the longest x4 1.23 us: block_step(): decay_sum = jnp.cumsum(log_forget, axis=-1)]
    psum x1, blocking collectives: 2.47 us -> 14.7 us  [shards(): sums = lax.psum(sums, ('inner', 'tp')) / channels]
    rev x6 -> x0, local copies, waits for them, and re-layouts: 11.7 us -> none  [the longest x1 9.42 us: memory_branch(): jnp.flip(finish(back_queries, numerator, denominator, running, decay_sum,...]
  transfers between devices with their start and end apart: 11 -> 8, of which waited for: 9 -> 5; matrix products, arithmetic and copies ran while one was open for 7% -> 33% of each run, Pallas kernels for 0% -> 0%
where the time goes in v1:
time: 262 us; the launch traced here: 260 us
  waiting for transfers between devices  62.4 us (24%)
  blocking collectives  50.6 us (19%)
  matrix products  38.3 us (15%)
  other arithmetic  33.8 us (13%)
  between operations  33.3 us (13%)
  local copies, waits for them, and re-layouts  31.9 us (12%)
  starting transfers between devices  9.99 us (4%)
    all_gather x1, waiting for transfers between devices, gather_inputs(): lax.all_gather(packed.reshape(inner * depth, -1), 'outer', axis=0, tiled=...  43.8 us
    all_to_all x1, blocking collectives, gather_inputs(): lax.all_to_all(packed, 'inner', split_axis=0, concat_axis=0, tiled=True)  27.6 us
    dot_general x5, matrix products, project(): jnp.dot(normed, weights[:, i * width:(i + 1) * width], preferred_element_...  15.3 us
    unnamed x30, local copies, waits for them, and re-layouts  15 us
    psum x1, blocking collectives, shards(): sums = lax.psum(sums, ('inner', 'tp')) / channels  14.7 us
    another operation x9, other arithmetic  12.9 us
    all_gather x1, blocking collectives, gather_inputs(): lax.all_gather(extra, 'inner', axis=0, tiled=True)  8.41 us
    reduce_scatter x1, waiting for transfers between devices, shards(): lax.psum_scatter(result.astype(jnp.bfloat16), 'tp', scatter_dimension=0,...  7.49 us
  transfers between devices with their start and end apart: 8, of which 5 were waited for; matrix products, arithmetic and copies ran while one was open for 33% of the time, Pallas kernels for 0%

profile of v1, /device:TPU:0, one launch (start us, length us, event | category | flops | bytes accessed | tf_op | source)
XLA Modules:
  0.0 260.4 jit_solution(12544550280953468704)
XLA Ops:
  7.3 1.1 copy.89
  8.4 1.1 copy.90
  9.6 1.1 copy.91
  10.7 1.1 copy.92
  11.8 1.1 copy.93
  13.2 27.6 %all_to_all.40 = bf16[4,128,1280]{1,2,0:T(8,128)(2,1)S(1)} all-to-all(bf16[4,128,1280]{1,2,0:T(8,128)(2,1)S(1)} %bitcast.226), channel_id=1, replica_groups=mesh['outer'=4,'inner'=4,'tp'=2] {'inner'}, dimensions={0} | all-to-all | bytes 2621440 | tf_op jit(solution)/shard_map/all_to_all | solution.py:39
  40.8 1.4 copy.94
  44.9 8.4 %all_gather.21 = f32[1024,16]{0,1:T(8,128)S(1)} all-gather(f32[256,16]{0,1:T(8,128)S(1)} %copy-done.5), channel_id=1, replica_groups=mesh['outer'=4,'inner'=4,'tp'=2] {'inner'}, dimensions={0}, use_global_device_ids=true | all-gather | bytes 81920 | tf_op jit(solution)/shard_map/all_gather | solution.py:41
  53.3 1.2 fusion.129
  54.5 1.4 constant_dynamic-slice_fusion
  56.0 4.6 %all-gather.8.cloned.1.call-done = bf16[2048,1024]{1,0:T(8,128)(2,1)} async-done(((bf16[256,1024]{1,0:T(8,128)(2,1)}), bf16[2048,1024]{1,0:T(8,128)(2,1)}) %all-gather.8.cloned.1.call-update) | async-done | bytes 4194320 | tf_op jit(solution)/shard_map/all_gather | solution.py:30
  60.6 3.2 %multiply_reduce_fusion = f32[4,256]{1,0:T(4,128)S(1)} fusion(bf16[4,2,256,1024]{3,2,1,0:T(8,128)(2,1)} %bitcast.220), kind=kLoop, calls=%fused_computation.2 | loop fusion | flops 6290432 | bytes 4198400 | tf_op jit(solution)/shard_map/reduce_sum | solution.py:134
  64.0 1.1 bitcast_convert_fusion
  65.1 8.8 %multiply_convert_fusion = (bf16[4,2,256,1024]{3,1,2,0:T(2,128)(2,1)S(1)}, f32[4,2,256,1024]{3,1,2,0:T(2,128)}) fusion(f32[2,1024]{1,0:T(2,128)S(1)} %mul.675, f32[4,256]{1,0:T(4,128)S(1)} %get-tuple-element.73, f32[4,2,256,1024]{3,2,1,0:T(8,128)S(1)} %bitcast_convert_fusion), kind=kLoop, calls=%fused_computation | loop fusion | flops 6291456 | bytes 20983808 | tf_op jit(solution)/shard_map/convert.4
  73.9 1.4 copy.108
  75.3 1.2 convolution_add_fusion.1
  76.6 1.2 reduce-window.34
  78.3 1.6 reduce-window.36
  106.0 7.5 %copy.106 = f32[128,8,2,1024]{3,1,2,0:T(8,128)S(1)} copy(f32[128,8,2,1024]{3,2,1,0:T(2,128)} %bitcast.218) | data formatting | bytes 16777216
  113.7 2.7 %multiply_convert_fusion.1 = bf16[1024,2048]{1,0:T(8,128)(2,1)} fusion(f32[1024,2048]{1,0:T(8,128)S(1)} %bitcast.219, f32[2048]{0:T(1024)S(1)} %copy-done.4, f32[1024]{0:T(1024)S(1)} %bitcast.249), kind=kLoop, calls=%fused_computation.1 | loop fusion | flops 6291456 | bytes 12595200 | tf_op jit(solution)/shard_map/convert_element_type | solution.py:135
  116.4 43.8 %all-gather.6.cloned.1.call-done = bf16[2048,1280]{1,0:T(8,128)(2,1)} async-done(((bf16[512,1280]{1,0:T(8,128)(2,1)}), bf16[2048,1280]{1,0:T(8,128)(2,1)}) %all-gather.6.cloned.1.call-update) | async-done | bytes 5242896 | tf_op jit(solution)/shard_map/all_gather | solution.py:40
  160.2 4.1 %convolution_convert_fusion.1 = bf16[1024,256]{1,0:T(8,128)(2,1)S(1)} fusion(bf16[1024,2048]{1,0:T(8,128)(2,1)} %multiply_convert_fusion.1, bf16[2048,1280]{1,0:T(8,128)(2,1)} %all-gather.6.cloned.1.call-done), kind=kOutput, calls=%fused_computation.33 | convolution fusion | flops 1074003968 | bytes 5767168 | tf_op jit(solution)/shard_map/dot_general | solution.py:156
  164.3 2.5 fusion.24
  168.0 2.5 fusion.22
  170.5 2.5 fusion.23
  173.0 1.3 collective-permute-start
  174.3 1.3 collective-permute-start.1
  176.7 3.7 %convolution_convert_fusion = bf16[1024,256]{1,0:T(8,128)(2,1)S(1)} fusion(bf16[1024,2048]{1,0:T(8,128)(2,1)} %multiply_convert_fusion.1, bf16[2048,1280]{1,0:T(8,128)(2,1)} %all-gather.6.cloned.1.call-done), kind=kOutput, calls=%fused_computation.32 | convolution fusion | flops 1074003968 | bytes 5767168 | tf_op jit(solution)/shard_map/dot_general | solution.py:156
  180.5 0.9 concatenate.9
  181.5 4.5 %fusion.120 = (f32[1024]{0:T(1024)S(1)}, f32[1024]{0:T(1024)S(1)}, f32[1024,256]{1,0:T(8,128)S(1)}) fusion(f32[1054,256]{1,0:T(8,128)S(1)} %convert_element_type.488, f32[256]{0:T(256)S(1)} %bitcast.271, f32[256]{0:T(256)S(1)} %bitcast.273, f32[256]{0:T(256)S(1)} %bitcast.274, f32[256]{0:T(256)S(1)} %bitcast.275, f32[256]{0:T(256)S(1)} %bitcast.276, ...), kind=kLoop, calls=%fused_computation.252 | loop fusion | flops 16775168 | bytes 33594368 | tf_op jit(solution)/shard_map/reduce_sum | solution.py:203
  186.0 14.7 %psum.7 = f32[2,1024]{1,0:T(2,128)S(1)} all-reduce(f32[2,1024]{1,0:T(2,128)S(1)} %pad_maximum_fusion.1), channel_id=1, replica_groups=mesh['outer'=4,'inner'=4,'tp'=2] {'inner','tp'}, use_global_device_ids=true, to_apply=%region_3.4 | all-reduce | flops 2048 | bytes 16384 | tf_op jit(solution)/shard_map/psum | solution.py:204
  201.2 1.0 copy.95
  202.2 3.7 %all-to-all-start.1 = ((bf16[4,256,256]{1,2,0:T(8,128)(2,1)}), bf16[4,256,256]{1,2,0:T(8,128)(2,1)S(1)}, u32[]{:S(2)}, u32[]{:S(2)}) async-start(bf16[4,256,256]{1,2,0:T(8,128)(2,1)} %copy.95), calls=%async_computation.1 | async-start | bytes 1048576 | tf_op jit(solution)/shard_map/all_to_all | solution.py:221
  205.9 1.6 all-gather.10.cloned.1.call-done
  207.5 1.3 slice_bitcast_fusion
  212.9 0.8 fusion.107
  215.1 4.2 %fusion.3 = (f32[1024]{0:T(1024)S(1)}, f32[1024]{0:T(1024)S(1)}, f32[1024,1024]{0,1:T(8,128)S(1)}) fusion(f32[1024]{0:T(1024)S(1)} %get-tuple-element.12, f32[1024]{0:T(1024)S(1)} %get-tuple-element.22, f32[1024]{0:T(1024)S(1)} %get-tuple-element.16, f32[1024]{0:T(1024)S(1)} %get-tuple-element.20, bf16[1024,256]{1,0:T(8,128)(2,1)S(1)} %convolution_convert_fusion, ...), kind=kOutput, calls=%fused_computation.11 | convolution fusion | flops 550500352 | bytes 5267456 | tf_op jit(solution)/shard_map/htd,hsd->hts/dot_general | solution.py:180
  220.0 2.2 fusion.15
  222.9 2.2 fusion.18
  225.3 0.8 fusion.108
  226.3 1.8 fusion.13
  228.1 1.2 multiply_reduce_fusion.1
  229.6 1.0 copy.102
  230.6 3.6 %all-to-all-start.2 = ((bf16[4,256,256]{1,2,0:T(8,128)(2,1)}), bf16[4,256,256]{1,2,0:T(8,128)(2,1)S(1)}, u32[]{:S(2)}, u32[]{:S(2)}) async-start(bf16[4,256,256]{1,2,0:T(8,128)(2,1)} %copy.102), calls=%async_computation.2 | async-start | bytes 1048576 | tf_op jit(solution)/shard_map/all_to_all | solution.py:221
  234.2 3.5 %fusion.133 = f32[256,2048]{1,0:T(8,128)S(1)} fusion(bf16[256,1024]{0,1:T(8,128)(2,1)S(1)} %bitcast.235, bf16[1024,2048]{1,0:T(8,128)(2,1)} %param.30), kind=kOutput, calls=%fused_computation.260 | convolution fusion | flops 1073741824 | bytes 6815744 | tf_op jit(solution)/shard_map/dot_general | solution.py:223
  237.6 4.2 %all-to-all-done.2 = bf16[4,256,256]{1,2,0:T(8,128)(2,1)S(1)} async-done(((bf16[4,256,256]{1,2,0:T(8,128)(2,1)}), bf16[4,256,256]{1,2,0:T(8,128)(2,1)S(1)}, u32[]{:S(2)}, u32[]{:S(2)}) %all-to-all-start.2) | async-done | bytes 524320 | tf_op jit(solution)/shard_map/all_to_all | solution.py:221
  241.8 4.5 %fusion = bf16[256,2048]{1,0:T(8,128)(2,1)} fusion(f32[256,2048]{1,0:T(8,128)S(1)} %fusion.133, bf16[256,1024]{0,1:T(8,128)(2,1)S(1)} %bitcast.236, bf16[1024,2048]{1,0:T(8,128)(2,1)} %param.31), kind=kOutput, calls=%fused_computation.8 | convolution fusion | flops 1074790400 | bytes 7864320 | tf_op jit(solution)/shard_map/dot_general | solution.py:224
  246.3 7.5 %reduce-scatter.2.cloned.1.call-done = bf16[128,2048]{1,0:T(8,128)(2,1)} async-done(((bf16[256,2048]{1,0:T(8,128)(2,1)}), bf16[128,2048]{1,0:T(8,128)(2,1)}) %reduce-scatter.2.cloned.1.call-update) | async-done | bytes 524304 | tf_op jit(solution)/shard_map/reduce_scatter | solution.py:225
  (130 shorter events, 21.1 us)
Async XLA Ops:
  6.5 49.4 %copy-start = (bf16[2048,32]{0,1:T(8,128)(2,1)S(1)}, bf16[2048,32]{0,1:T(8,128)(2,1)}, u32[]{:S(2)}) copy-start(bf16[2048,32]{0,1:T(8,128)(2,1)} %param.26) | copy-start | bytes 393220
  6.5 54.0 %all-gather.8.cloned.1.call-start = ((), (), s32[]{:S(2)}) async-start(), calls=%async_computation.6 | async-start | bytes 4718592 | tf_op jit(solution)/shard_map/all_gather | solution.py:30
  7.3 153.0 %all-gather.6.cloned.1.call-start = ((), (), s32[]{:S(2)}) async-start(), calls=%async_computation.4 | async-start | bytes 6553600 | tf_op jit(solution)/shard_map/all_gather | solution.py:40
  13.1 29.2 %copy-start.4 = (f32[2048]{0:T(1024)S(1)}, f32[2048]{0:T(1024)}, u32[]{:S(2)}) copy-start(f32[2048]{0:T(1024)} %param.17) | copy-start | bytes 24580
  13.1 30.8 %copy-start.6 = (f32[32]{0:T(128)S(1)}, f32[32]{0:T(128)}, u32[]{:S(2)}) copy-start(f32[32]{0:T(128)} %param.27) | copy-start | bytes 388
  13.1 31.8 %copy-start.5 = (f32[256,16]{0,1:T(8,128)S(1)}, f32[256,16]{0,1:T(8,128)}, u32[]{:S(2)}) copy-start(f32[256,16]{0,1:T(8,128)} %param.28) | copy-start | bytes 49156
  42.2 165.3 %all-gather.10.cloned.1.call-start = ((), (), s32[]{:S(2)}) async-start(), calls=%async_computation.7 | async-start | bytes 1392640 | tf_op jit(solution)/shard_map/all_gather | solution.py:172
  60.6 3.4 %copy-start.2 = (bf16[2048,1024]{1,0:T(8,128)(2,1)S(1)}, bf16[2048,1024]{1,0:T(8,128)(2,1)}, u32[]{:S(2)}) copy-start(bf16[2048,1024]{1,0:T(8,128)(2,1)} %all-gather.8.cloned.1.call-done) | copy-start | bytes 12582916
  160.2 4.1 %copy-start.3 = (bf16[1024,2048]{1,0:T(8,128)(2,1)S(1)}, bf16[1024,2048]{1,0:T(8,128)(2,1)}, u32[]{:S(2)}) copy-start(bf16[1024,2048]{1,0:T(8,128)(2,1)} %multiply_convert_fusion.1) | copy-start | bytes 12582916
  166.9 1.1 copy-start.7
  173.0 7.4 %collective-permute-start = (bf16[15,256]{1,0:T(8,128)(2,1)S(1)}, bf16[15,256]{1,0:T(8,128)(2,1)S(1)}, u32[]{:S(2)}, u32[]{:S(2)}) collective-permute-start(bf16[15,256]{1,0:T(8,128)(2,1)S(1)} %get-tuple-element.31), channel_id=1, source_target_pairs={{0,8},{8,16},{16,24},{1,9},{9,17},{17,25},{2,10},{10,18},{18,26},{... | collective-permute-start | bytes 23048 | tf_op jit(solution)/shard_map/ppermute | solution.py:176
  174.3 6.1 %collective-permute-start.1 = (bf16[15,256]{1,0:T(8,128)(2,1)S(1)}, bf16[15,256]{1,0:T(8,128)(2,1)S(1)}, u32[]{:S(2)}, u32[]{:S(2)}) collective-permute-start(bf16[15,256]{1,0:T(8,128)(2,1)S(1)} %get-tuple-element.30), channel_id=1, source_target_pairs={{8,0},{16,8},{24,16},{9,1},{17,9},{25,17},{10,2},{18,10},{26,18},{... | collective-permute-start | bytes 23048 | tf_op jit(solution)/shard_map/ppermute | solution.py:177
  202.2 28.4 %all-to-all-start.1 = ((bf16[4,256,256]{1,2,0:T(8,128)(2,1)}), bf16[4,256,256]{1,2,0:T(8,128)(2,1)S(1)}, u32[]{:S(2)}, u32[]{:S(2)}) async-start(bf16[4,256,256]{1,2,0:T(8,128)(2,1)} %copy.95), calls=%async_computation.1 | async-start | bytes 1048576 | tf_op jit(solution)/shard_map/all_to_all | solution.py:221
  225.2 2.9 %copy-start.8 = (f32[1024,256]{1,0:T(8,128)S(1)}, f32[1024,256]{1,0:T(8,128)}, u32[]{:S(2)}) copy-start(f32[1024,256]{1,0:T(8,128)} %fusion.18) | copy-start | bytes 3145732
  230.6 11.2 %all-to-all-start.2 = ((bf16[4,256,256]{1,2,0:T(8,128)(2,1)}), bf16[4,256,256]{1,2,0:T(8,128)(2,1)S(1)}, u32[]{:S(2)}, u32[]{:S(2)}) async-start(bf16[4,256,256]{1,2,0:T(8,128)(2,1)} %copy.102), calls=%async_computation.2 | async-start | bytes 1048576 | tf_op jit(solution)/shard_map/all_to_all | solution.py:221
  234.2 19.6 %reduce-scatter.2.cloned.1.call-start = ((), (), s32[]{:S(2)}) async-start(), calls=%async_computation.5 | async-start | bytes 1572864 | tf_op jit(solution)/shard_map/reduce_scatter | solution.py:225
  241.8 12.0 %copy-start.1 = (bf16[2048,32]{0,1:T(8,128)(2,1)S(1)}, bf16[2048,32]{0,1:T(8,128)(2,1)}, u32[]{:S(2)}) copy-start(bf16[2048,32]{0,1:T(8,128)(2,1)} %param.26) | copy-start | bytes 393220
Sparse Core Ops, SparseCore 0:
  9.2 51.3 all-gather.7
  62.1 98.0 all-gather.5
  176.8 30.6 all-gather.9
  246.5 7.3 reduce-scatter.1

commit v2 on v1

--- a/solution.py
+++ b/solution.py
@@ -1,8 +1,11 @@
+import functools
 import math
 
 import jax
 import jax.numpy as jnp
 from jax import lax
+from jax.experimental import pallas as pl
+from jax.experimental.pallas import tpu as pltpu
 from jax.sharding import Mesh, PartitionSpec as P
 
 MEMORY_HEADS = 8
@@ -23,6 +26,192 @@
 
 def whole_of(a, b, c):
     return a.astype(jnp.float32) + b.astype(jnp.float32) + c.astype(jnp.float32)
+
+
+MESH = pl.DeviceIdType.MESH
+
+
+def exchange_kernel(outer, inner, tp, count, *refs):
+    tokens, extra = refs[:2]
+    weights = refs[2 : 2 + count]
+    whole, extras, pieces, stage_w, stage_t, stage_e = refs[2 + count : 8 + count]
+    local, a2a_s, a2a_r, tok_s, tok_r, ext_s, ext_r, half_s, half_r, ring_s, ring_r = refs[8 + count :]
+    o, i, t = lax.axis_index("outer"), lax.axis_index("inner"), lax.axis_index("tp")
+    right, left = lax.rem(o + 1, outer), lax.rem(o + outer - 1, outer)
+    rows, half = tokens.shape
+    depth = weights[0].shape[0]
+    width = pieces.shape[2]
+
+    barrier = pltpu.get_barrier_semaphore()
+    greeted = [(o, lax.rem(i + k, inner), t) for k in range(1, inner)]
+    greeted += [(o, i, lax.rem(t + k, tp)) for k in range(1, tp)]
+    greeted += [(right, i, t), (left, i, t)]
+    for device in greeted:
+        pl.semaphore_signal(barrier, inc=1, device_id=device, device_id_type=MESH)
+    pl.semaphore_wait(barrier, len(greeted))
+
+    def columns(index):
+        return pl.ds(pl.multiple_of(index * width, width), width)
+
+    def piece(owner, index):
+        start = pl.multiple_of((owner * inner + index) * depth, depth)
+        return pieces.at[:, pl.ds(start, depth), :]
+
+    def block(index, core):
+        return whole.at[
+            pl.ds(pl.multiple_of(index * rows, rows), rows),
+            pl.ds(pl.multiple_of(core * half, half), half),
+        ]
+
+    def remote(src, dst, send, recv, device):
+        return pltpu.make_async_remote_copy(
+            src_ref=src, dst_ref=dst, send_sem=send, recv_sem=recv,
+            device_id=device, device_id_type=MESH,
+        )
+
+    sends = []
+
+    def start(copy):
+        copy.start()
+        sends.append(copy)
+
+    staged = [
+        pltpu.make_async_copy(weights[j].at[:, columns(i)], stage_w.at[j], local.at[j])
+        for j in range(count)
+    ]
+    staged.append(pltpu.make_async_copy(tokens, stage_t, local.at[count]))
+    staged.append(pltpu.make_async_copy(extra, stage_e, local.at[count + 1]))
+    for copy in staged:
+        copy.start()
+
+    def a2a(k, j):
+        peer = lax.rem(i + k, inner)
+        start_row = pl.multiple_of((o * inner + i) * depth, depth)
+        return remote(
+            weights[j].at[:, columns(peer)], pieces.at[j, pl.ds(start_row, depth), :],
+            a2a_s.at[k - 1, j], a2a_r.at[k - 1, j], (o, peer, t),
+        )
+
+    def ring(way, distance, k, src=None):
+        index = lax.rem(i + inner - k, inner)
+        back = outer - (distance - 1) if way == 0 else distance - 1
+        owner = lax.rem(o + back, outer)
+        target = right if way == 0 else left
+        return remote(
+            piece(owner, index) if src is None else src, piece(owner, index),
+            ring_s.at[way, distance - 1, k], ring_r.at[way, distance - 1, k], (target, i, t),
+        )
+
+    far = outer // 2
+
+    def uses(way, distance, k):
+        if 2 * distance < outer:
+            return True
+        return (k < inner // 2) == (way == 0)
+
+    def tok(k):
+        peer = lax.rem(i + k, inner)
+        return remote(tokens, block(i, t), tok_s.at[k - 1], tok_r.at[k - 1], (o, peer, t))
+
+    def ext(k):
+        peer = lax.rem(i + k, inner)
+        return remote(extra, extras.at[i], ext_s.at[k - 1], ext_r.at[k - 1], (o, peer, t))
+
+    def hand(k, c, src=None):
+        index = lax.rem(i + inner - k, inner)
+        other = lax.rem(t + c, tp)
+        return remote(
+            block(index, t) if src is None else src, block(index, t),
+            half_s.at[k, c - 1], half_r.at[k, c - 1], (o, i, other),
+        )
+
+    for k in range(1, inner):
+        for j in range(count):
+            start(a2a(k, j))
+        start(ext(k))
+    for j in range(count):
+        staged[j].wait()
+    for way in range(2):
+        start(ring(way, 1, 0, stage_w))
+    for k in range(1, inner):
+        start(tok(k))
+    for c in range(1, tp):
+        start(hand(0, c, tokens))
+    staged[count].wait()
+    staged[count + 1].wait()
+    start_own = [
+        pltpu.make_async_copy(stage_w, piece(o, i), local.at[0]),
+        pltpu.make_async_copy(stage_t, block(i, t), local.at[1]),
+        pltpu.make_async_copy(stage_e, extras.at[i], local.at[2]),
+    ]
+    for copy in start_own:
+        copy.start()
+
+    def relay(distance, k):
+        for way in range(2):
+            if uses(way, distance, k):
+                ring(way, distance, k).wait_recv()
+                if distance < far and uses(way, distance + 1, k):
+                    start(ring(way, distance + 1, k))
+
+    for k in range(1, inner):
+        for j in range(count):
+            a2a(k, j).wait_recv()
+        for way in range(2):
+            start(ring(way, 1, k))
+        relay(1, k - 1)
+    relay(1, inner - 1)
+    for k in range(1, inner):
+        tok(k).wait_recv()
+        for c in range(1, tp):
+            start(hand(k, c))
+    for distance in range(2, far + 1):
+        for k in range(inner):
+            relay(distance, k)
+    for k in range(1, inner):
+        ext(k).wait_recv()
+    for k in range(inner):
+        for c in range(1, tp):
+            hand(k, c).wait_recv()
+    for copy in start_own:
+        copy.wait()
+    for copy in sends:
+        copy.wait_send()
+
+
+def exchange(tokens, weights, extra, outer, inner, tp):
+    rows, half = tokens.shape
+    depth, columns = weights[0].shape
+    width = columns // inner
+    count = len(weights)
+    turned = extra.T
+    dma = pltpu.SemaphoreType.DMA
+    far = outer // 2
+    any_space = pl.BlockSpec(memory_space=pl.ANY)
+    whole, extras, pieces = pl.pallas_call(
+        functools.partial(exchange_kernel, outer, inner, tp, count),
+        out_shape=(
+            jax.ShapeDtypeStruct((inner * rows, tp * half), tokens.dtype),
+            jax.ShapeDtypeStruct((inner,) + turned.shape, turned.dtype),
+            jax.ShapeDtypeStruct((count, outer * inner * depth, width), weights[0].dtype),
+        ),
+        in_specs=[any_space] * (2 + count),
+        out_specs=(any_space,) * 3,
+        scratch_shapes=[
+            pltpu.VMEM((count, depth, width), weights[0].dtype),
+            pltpu.VMEM((rows, half), tokens.dtype),
+            pltpu.VMEM(turned.shape, turned.dtype),
+            dma((count + 2,)),
+            dma((inner - 1, count)), dma((inner - 1, count)),
+            dma((inner - 1,)), dma((inner - 1,)),
+            dma((inner - 1,)), dma((inner - 1,)),
+            dma((inner, tp - 1)), dma((inner, tp - 1)),
+            dma((2, far, inner)), dma((2, far, inner)),
+        ],
+        compiler_params=pltpu.CompilerParams(collective_id=0, has_side_effects=True),
+    )(tokens, turned, *weights)
+    extras = jnp.transpose(extras, (1, 0, 2)).reshape(turned.shape[0], inner * rows)
+    return whole, pieces, extras
 
 
 def gather_inputs(tokens, weights, extra, inner):
@@ -38,8 +227,9 @@
     if inner > 1:
         packed = lax.all_to_all(packed, "inner", split_axis=0, concat_axis=0, tiled=True)
     pieces = lax.all_gather(packed.reshape(inner * depth, -1), "outer", axis=0, tiled=True)
+    pieces = pieces.reshape(-1, len(weights), width).transpose(1, 0, 2)
     extras = lax.all_gather(extra, "inner", axis=0, tiled=True) if inner > 1 else extra
-    return whole, pieces, extras
+    return whole, pieces, extras.T
 
 
 def local_state(keys, values, shifted, level, total, scale):
@@ -124,10 +314,11 @@
         width = gain.shape[0]
         heads = mgain.shape[0] // HEAD
         first = (lax.axis_index("tp") * inner + lax.axis_index("inner")) * heads
-        whole, weights, extras = gather_inputs(
-            tokens, (query_weight, key_weight, value_weight, glu_value, glu_gate),
-            log_decay_extra, inner,
-        )
+        stacked = (query_weight, key_weight, value_weight, glu_value, glu_gate)
+        if inner > 1 and tp > 1 and outer > 2:
+            whole, weights, extras = exchange(tokens, stacked, log_decay_extra, outer, inner, tp)
+        else:
+            whole, weights, extras = gather_inputs(tokens, stacked, log_decay_extra, inner)
         rows = whole.shape[0]
         wide = whole.astype(jnp.float32)
         normed = (
@@ -142,8 +333,8 @@
             preferred_element_type=jnp.float32,
         ).reshape(4, heads, rows) + own_bias[:, :, None]
         own_extra = lax.dynamic_slice_in_dim(
-            extras.reshape(rows, 2, MEMORY_HEADS), first, heads, 2
-        ).transpose(1, 2, 0)
+            extras.reshape(2, MEMORY_HEADS, rows), first, heads, 1
+        )
         lf = jax.nn.log_sigmoid(gates[1::2]) + own_extra
         decay_f = jnp.cumsum(lf[0], axis=-1)
         decay_b = lax.cumsum(lf[1], axis=1, reverse=True)
@@ -153,10 +344,7 @@
         running_b = lax.cummax(shifted_b, axis=1, reverse=True)
 
         def project(i):
-            return jnp.dot(
-                normed, weights[:, i * width : (i + 1) * width],
-                preferred_element_type=jnp.float32,
-            )
+            return jnp.dot(normed, weights[i], preferred_element_type=jnp.float32)
 
         def heads_first(x):
             return jnp.transpose(x.reshape(rows, heads, HEAD), (1, 0, 2)).astype(jnp.bfloat16)

time: 262 us -> 242 us (0.924)
  Pallas kernels: 0 us -> 92.1 us
  waiting for transfers between devices: 62.4 us -> 11.9 us
  blocking collectives: 50.6 us -> 12.5 us
  local copies, waits for them, and re-layouts: 31.9 us -> 19.2 us
  other arithmetic: 33.8 us -> 22 us
  starting transfers between devices: 9.99 us -> 13.5 us
    pallas_call x0 -> x1, Pallas kernels: none -> 92.1 us  [exchange(): pl.pallas_call(functools.partial(exchange_kernel, outer, inner, tp, count...]
    all_gather x2 -> x0, waiting for transfers between devices: 48.4 us -> none  [the longest x1 43.8 us: gather_inputs(): lax.all_gather(packed.reshape(inner * depth, -1), 'outer', axis=0, tiled=...]
    all_to_all x1 -> x0, blocking collectives: 27.6 us -> none  [gather_inputs(): lax.all_to_all(packed, 'inner', split_axis=0, concat_axis=0, tiled=True)]
    unnamed x30 -> x14, local copies, waits for them, and re-layouts: 15 us -> 2.2 us
    another operation x9 -> x8, other arithmetic: 12.9 us -> 4.11 us
    all_gather x1 -> x0, blocking collectives: 8.41 us -> none  [gather_inputs(): lax.all_gather(extra, 'inner', axis=0, tiled=True)]
    ppermute x1, starting transfers between devices: 1.29 us -> 4.55 us  [shards(): lax.ppermute(glu[rows - reach:], 'outer', [(i, i + 1) for i in range(oute...]
  transfers between devices with their start and end apart: 8 -> 6, of which waited for: 5 -> 2; matrix products, arithmetic and copies ran while one was open for 33% -> 19% of each run, Pallas kernels for 0% -> 0%
where the time goes in v2:
time: 242 us; the launch traced here: 241 us
  Pallas kernels  92.1 us (38%)
  matrix products  36.3 us (15%)
  between operations  34 us (14%)
  other arithmetic  22 us (9%)
  local copies, waits for them, and re-layouts  19.2 us (8%)
  starting transfers between devices  13.5 us (6%)
  blocking collectives  12.5 us (5%)
  waiting for transfers between devices  11.9 us (5%)
    pallas_call x1, Pallas kernels, exchange(): pl.pallas_call(functools.partial(exchange_kernel, outer, inner, tp, count...  92.1 us
    dot_general x5, matrix products, project(): return jnp.dot(normed, weights[i], preferred_element_type=jnp.float32)  16.5 us
    psum x1, blocking collectives, shards(): sums = lax.psum(sums, ('inner', 'tp')) / channels  12.5 us
    reduce_scatter x1, waiting for transfers between devices, shards(): lax.psum_scatter(result.astype(jnp.bfloat16), 'tp', scatter_dimension=0,...  7.96 us
    all_to_all x2, starting transfers between devices, back(): return lax.all_to_all(x, 'inner', split_axis=0, concat_axis=1, tiled=True)  7.61 us
  transfers between devices with their start and end apart: 6, of which 2 were waited for; matrix products, arithmetic and copies ran while one was open for 19% of the time, Pallas kernels for 0%

profile of v2, /device:TPU:0, one launch (start us, length us, event | category | flops | bytes accessed | tf_op | source)
XLA Modules:
  0.0 241.4 jit_solution(4731296346340131956)
XLA Ops:
  6.5 0.8 reshape.1293
  7.6 92.1 %shard_map.154 = (bf16[1024,2048]{1,0:T(8,128)(2,1)}, f32[4,16,256]{2,1,0:T(8,128)}, bf16[5,2048,256]{2,1,0:T(8,128)(2,1)}) custom-call(bf16[256,1024]{1,0:T(8,128)(2,1)} %refs_0_.1, f32[16,256]{1,0:T(8,128)} %bitcast.228, bf16[128,1024]{1,0:T(8,128)(2,1)} %refs_2_.1, bf16[128,1024]{1,0:T(8,128)(2,1)} %refs_3_.1, bf16[128,1024]{1,0:T(8,128)(2,1)} %refs_4_.1, ...), custom_call_target="tpu_custom_call" | custom-call | tf_op jit(solution)/shard_map/pallas_call | solution.py:191
  99.7 0.9 copy.49
  100.7 3.2 %fusion = f32[1024]{0:T(1024)S(1)} fusion(bf16[1024,2048]{1,0:T(8,128)(2,1)} %get-tuple-element.8), kind=kLoop, calls=%fused_computation.2 | loop fusion | flops 6290432 | bytes 4198400 | tf_op jit(solution)/shard_map/reduce_sum | solution.py:325
  104.1 1.0 fusion.2
  105.1 2.0 copy-done.1
  107.1 1.2 convolution_add_fusion.1
  115.3 1.2 reduce-window.34
  122.9 1.6 reduce-window.36
  132.4 0.7 slice.500
  138.3 3.7 %convolution_convert_fusion.1 = bf16[1024,256]{1,0:T(8,128)(2,1)S(1)} fusion(bf16[1024,2048]{1,0:T(8,128)(2,1)} %copy-done.1, bf16[5,2048,256]{2,1,0:T(8,128)(2,1)} %get-tuple-element.9), kind=kOutput, calls=%fused_computation.35 | convolution fusion | flops 1074003968 | bytes 5767168 | tf_op jit(solution)/shard_map/dot_general | solution.py:347
  142.2 2.5 %fusion.27 = (f32[256]{0:T(256)S(1)}, f32[256]{0:T(256)S(1)}, bf16[1024,256]{1,0:T(8,128)(2,1)S(1)}) fusion(f32[1024]{0:T(1024)S(1)} %get-tuple-element.25, f32[1024]{0:T(1024)S(1)} %get-tuple-element.27, bf16[1024,2048]{1,0:T(8,128)(2,1)S(1)} %copy-done.2, bf16[5,2048,256]{2,1,0:T(8,128)(2,1)} %get-tuple-element.9), kind=kOutput, calls=%fused_computation.37 | convolution fusion | flops 1075314176 | bytes 5777408 | tf_op jit(solution)/shard_map/dot_general | solution.py:347
  146.2 0.7 pad_maximum_fusion
  147.0 3.9 %fusion.25 = f32[1024,256]{1,0:T(8,128)S(1)} fusion(bf16[1024,2048]{1,0:T(8,128)(2,1)} %copy-done.1, bf16[5,2048,256]{2,1,0:T(8,128)(2,1)} %get-tuple-element.9), kind=kOutput, calls=%fused_computation.32 | convolution fusion | flops 1074528256 | bytes 6291456 | tf_op jit(solution)/shard_map/dot_general | solution.py:347
  150.9 2.7 %fusion.26 = bf16[1024,256]{1,0:T(8,128)(2,1)S(1)} fusion(f32[1024,256]{1,0:T(8,128)S(1)} %fusion.25, bf16[1024,2048]{1,0:T(8,128)(2,1)S(1)} %copy-done.3, bf16[5,2048,256]{2,1,0:T(8,128)(2,1)} %get-tuple-element.9), kind=kOutput, calls=%fused_computation.33 | convolution fusion | flops 1074266112 | bytes 6815744 | tf_op jit(solution)/shard_map/dot_general | solution.py:347
  153.6 1.3 collective-permute-start.1
  154.9 4.5 %collective-permute-start = (bf16[15,256]{1,0:T(8,128)(2,1)S(1)}, bf16[15,256]{1,0:T(8,128)(2,1)S(1)}, u32[]{:S(2)}, u32[]{:S(2)}) collective-permute-start(bf16[15,256]{1,0:T(8,128)(2,1)S(1)} %get-tuple-element.35), channel_id=1, source_target_pairs={{0,8},{8,16},{16,24},{1,9},{9,17},{17,25},{2,10},{10,18},{18,26},{... | collective-permute-start | bytes 23048 | tf_op jit(solution)/shard_map/ppermute | solution.py:364
  159.4 3.7 %convolution_convert_fusion = bf16[1024,256]{1,0:T(8,128)(2,1)S(1)} fusion(bf16[1024,2048]{1,0:T(8,128)(2,1)} %copy-done.1, bf16[5,2048,256]{2,1,0:T(8,128)(2,1)} %get-tuple-element.9), kind=kOutput, calls=%fused_computation.34 | convolution fusion | flops 1074003968 | bytes 5767168 | tf_op jit(solution)/shard_map/dot_general | solution.py:347
  163.2 1.2 fusion.136
  164.4 1.3 constant_dynamic-slice_fusion
  165.8 0.8 dynamic_slice.22
  166.5 0.8 dynamic_slice.23
  167.3 0.8 dynamic_slice.27
  168.1 0.9 concatenate.9
  169.1 4.5 %fusion.127 = (f32[1024]{0:T(1024)S(1)}, f32[1024]{0:T(1024)S(1)}, f32[1024,256]{1,0:T(8,128)S(1)}) fusion(f32[1054,256]{1,0:T(8,128)S(1)} %convert_element_type.466, f32[256]{0:T(256)S(1)} %bitcast.250, f32[256]{0:T(256)S(1)} %bitcast.252, f32[256]{0:T(256)S(1)} %bitcast.253, f32[256]{0:T(256)S(1)} %bitcast.254, f32[256]{0:T(256)S(1)} %bitcast.255, ...), kind=kLoop, calls=%fused_computation.251 | loop fusion | flops 16775168 | bytes 33594368 | tf_op jit(solution)/shard_map/reduce_sum | solution.py:391
  173.6 12.5 %psum.7 = f32[2,1024]{1,0:T(2,128)S(1)} all-reduce(f32[2,1024]{1,0:T(2,128)S(1)} %pad_maximum_fusion.1), channel_id=1, replica_groups=mesh['outer'=4,'inner'=4,'tp'=2] {'inner','tp'}, use_global_device_ids=true, to_apply=%region_3.4 | all-reduce | flops 2048 | bytes 16384 | tf_op jit(solution)/shard_map/psum | solution.py:392
  186.6 1.0 copy.47
  187.6 3.5 %all-to-all-start = ((bf16[4,256,256]{1,2,0:T(8,128)(2,1)}), bf16[4,256,256]{1,2,0:T(8,128)(2,1)S(1)}, u32[]{:S(2)}, u32[]{:S(2)}) async-start(bf16[4,256,256]{1,2,0:T(8,128)(2,1)} %copy.47), calls=%async_computation | async-start | bytes 1048576 | tf_op jit(solution)/shard_map/all_to_all | solution.py:409
  191.1 1.3 slice_bitcast_fusion
  192.9 0.7 fusion.125
  193.5 0.7 exponential_select_fusion.1
  194.2 0.8 fusion.80
  195.6 0.6 fusion.85
  196.5 0.7 fusion.116
  197.5 0.8 fusion.115
  199.5 4.2 %fusion.6 = (f32[1024]{0:T(1024)S(1)}, f32[1024]{0:T(1024)S(1)}, f32[1024,1024]{0,1:T(8,128)S(1)}) fusion(f32[1024]{0:T(1024)S(1)} %get-tuple-element.18, f32[1024]{0:T(1024)S(1)} %get-tuple-element.28, f32[1024]{0:T(1024)S(1)} %get-tuple-element.22, f32[1024]{0:T(1024)S(1)} %get-tuple-element.26, bf16[1024,256]{1,0:T(8,128)(2,1)S(1)} %convolution_convert_fusion, ...), kind=kOutput, calls=%fused_computation.13 | convolution fusion | flops 550500352 | bytes 5267456 | tf_op jit(solution)/shard_map/htd,hsd->hts/dot_general | solution.py:368
  203.7 0.8 fusion.83
  204.4 0.6 fusion.88
  205.1 1.2 fusion.18
  206.3 1.2 fusion.21
  207.5 0.6 fusion.16
  208.1 1.3 multiply_reduce_fusion
  209.7 1.0 copy.54
  210.7 4.1 %all-to-all-start.1 = ((bf16[4,256,256]{1,2,0:T(8,128)(2,1)}), bf16[4,256,256]{1,2,0:T(8,128)(2,1)S(1)}, u32[]{:S(2)}, u32[]{:S(2)}) async-start(bf16[4,256,256]{1,2,0:T(8,128)(2,1)} %copy.54), calls=%async_computation.1 | async-start | bytes 1048576 | tf_op jit(solution)/shard_map/all_to_all | solution.py:409
  214.8 3.5 %fusion.140 = f32[256,2048]{1,0:T(8,128)S(1)} fusion(bf16[256,1024]{0,1:T(8,128)(2,1)S(1)} %bitcast.214, bf16[1024,2048]{1,0:T(8,128)(2,1)} %param.30), kind=kOutput, calls=%fused_computation.259 | convolution fusion | flops 1073741824 | bytes 6815744 | tf_op jit(solution)/shard_map/dot_general | solution.py:411
  218.3 3.8 %all-to-all-done.1 = bf16[4,256,256]{1,2,0:T(8,128)(2,1)S(1)} async-done(((bf16[4,256,256]{1,2,0:T(8,128)(2,1)}), bf16[4,256,256]{1,2,0:T(8,128)(2,1)S(1)}, u32[]{:S(2)}, u32[]{:S(2)}) %all-to-all-start.1) | async-done | bytes 524320 | tf_op jit(solution)/shard_map/all_to_all | solution.py:409
  222.1 4.5 %fusion.3 = bf16[256,2048]{1,0:T(8,128)(2,1)} fusion(f32[256,2048]{1,0:T(8,128)S(1)} %fusion.140, bf16[256,1024]{0,1:T(8,128)(2,1)S(1)} %bitcast.215, bf16[1024,2048]{1,0:T(8,128)(2,1)} %param.31), kind=kOutput, calls=%fused_computation.10 | convolution fusion | flops 1074790400 | bytes 7864320 | tf_op jit(solution)/shard_map/dot_general | solution.py:412
  226.6 8.0 %reduce-scatter.2.cloned.1.call-done = bf16[128,2048]{1,0:T(8,128)(2,1)} async-done(((bf16[256,2048]{1,0:T(8,128)(2,1)}), bf16[128,2048]{1,0:T(8,128)(2,1)}) %reduce-scatter.2.cloned.1.call-update) | async-done | bytes 524304 | tf_op jit(solution)/shard_map/reduce_scatter | solution.py:413
  (104 shorter events, 12.0 us)
Async XLA Ops:
  6.5 1.0 copy-start
  6.5 97.4 %copy-start.5 = (f32[2048]{0:T(1024)S(1)}, f32[2048]{0:T(1024)}, u32[]{:S(2)}) copy-start(f32[2048]{0:T(1024)} %param.17) | copy-start | bytes 24580
  6.5 184.5 %all-gather.3.cloned.1.call-start = ((), (), s32[]{:S(2)}) async-start(), calls=%async_computation.4 | async-start | bytes 1392640 | tf_op jit(solution)/shard_map/all_gather | solution.py:360
  100.6 3.5 %copy-start.4 = (bf16[1024,2048]{1,0:T(8,128)(2,1)S(1)}, bf16[1024,2048]{1,0:T(8,128)(2,1)}, u32[]{:S(2)}) copy-start(bf16[1024,2048]{1,0:T(8,128)(2,1)} %get-tuple-element.8) | copy-start | bytes 12582916
  105.1 2.0 copy-start.1
  132.3 9.9 %copy-start.2 = (bf16[1024,2048]{1,0:T(8,128)(2,1)S(1)}, bf16[1024,2048]{1,0:T(8,128)(2,1)}, u32[]{:S(2)}) copy-start(bf16[1024,2048]{1,0:T(8,128)(2,1)} %copy-done.1) | copy-start | bytes 12582916
  144.7 1.1 copy-start.6
  147.0 3.9 %copy-start.3 = (bf16[1024,2048]{1,0:T(8,128)(2,1)S(1)}, bf16[1024,2048]{1,0:T(8,128)(2,1)}, u32[]{:S(2)}) copy-start(bf16[1024,2048]{1,0:T(8,128)(2,1)} %copy-done.1) | copy-start | bytes 12582916
  153.6 14.5 %collective-permute-start.1 = (bf16[15,256]{1,0:T(8,128)(2,1)S(1)}, bf16[15,256]{1,0:T(8,128)(2,1)S(1)}, u32[]{:S(2)}, u32[]{:S(2)}) collective-permute-start(bf16[15,256]{1,0:T(8,128)(2,1)S(1)} %get-tuple-element.34), channel_id=1, source_target_pairs={{8,0},{16,8},{24,16},{9,1},{17,9},{25,17},{10,2},{18,10},{26,18},{... | collective-permute-start | bytes 23048 | tf_op jit(solution)/shard_map/ppermute | solution.py:365
  154.9 13.2 %collective-permute-start = (bf16[15,256]{1,0:T(8,128)(2,1)S(1)}, bf16[15,256]{1,0:T(8,128)(2,1)S(1)}, u32[]{:S(2)}, u32[]{:S(2)}) collective-permute-start(bf16[15,256]{1,0:T(8,128)(2,1)S(1)} %get-tuple-element.35), channel_id=1, source_target_pairs={{0,8},{8,16},{16,24},{1,9},{9,17},{17,25},{2,10},{10,18},{18,26},{... | collective-permute-start | bytes 23048 | tf_op jit(solution)/shard_map/ppermute | solution.py:364
  187.6 23.1 %all-to-all-start = ((bf16[4,256,256]{1,2,0:T(8,128)(2,1)}), bf16[4,256,256]{1,2,0:T(8,128)(2,1)S(1)}, u32[]{:S(2)}, u32[]{:S(2)}) async-start(bf16[4,256,256]{1,2,0:T(8,128)(2,1)} %copy.47), calls=%async_computation | async-start | bytes 1048576 | tf_op jit(solution)/shard_map/all_to_all | solution.py:409
  210.7 11.4 %all-to-all-start.1 = ((bf16[4,256,256]{1,2,0:T(8,128)(2,1)}), bf16[4,256,256]{1,2,0:T(8,128)(2,1)S(1)}, u32[]{:S(2)}, u32[]{:S(2)}) async-start(bf16[4,256,256]{1,2,0:T(8,128)(2,1)} %copy.54), calls=%async_computation.1 | async-start | bytes 1048576 | tf_op jit(solution)/shard_map/all_to_all | solution.py:409
  214.8 19.8 %reduce-scatter.2.cloned.1.call-start = ((), (), s32[]{:S(2)}) async-start(), calls=%async_computation.3 | async-start | bytes 1572864 | tf_op jit(solution)/shard_map/reduce_scatter | solution.py:413
Sparse Core Ops, SparseCore 0:
  147.1 30.3 all-gather.2
  226.7 7.7 reduce-scatter.1
